TPU v7x, 32 devices: a whole 2x2x4 slice. The times are simulated.
32 devices in a mesh: dp: 4 (over y, x), kv: 4 (over z), tp: 2 (over core).
Axes of the slice: x: 2, y: 2, z: 4, core: 2. Of those that a mesh axis runs over, the one named last changes fastest.
Arguments:
- pieces: bfloat16 [4096, 8, 2048], P(('kv', 'tp'), 'dp'), parts along dimension 1, may hold values from -6 to 6
- new_tokens: bfloat16 [256, 2048], P(('dp', 'kv', 'tp')), parts along dimension 0, may hold values from -6 to 6
- w_query: bfloat16 [2048, 1024], P(None, 'tp'), may hold values from -0.125 to 0.125
- w_key: bfloat16 [2048, 1024], P(None, 'tp'), may hold values from -0.125 to 0.125
- w_value: bfloat16 [2048, 2048], P(None, 'tp'), may hold values from -0.125 to 0.125
- w_decay: bfloat16 [2048, 1024], P(None, 'tp'), may hold values from -0.125 to 0.125
- decay_bias: float32 [1024], replicated, may hold values from 0 to 9
- norm_gain: float32 [2048], replicated, may hold values from 0.1 to 1.9
- head_gain: float32 [2048], replicated, may hold values from 0.1 to 1.9
- w_out: bfloat16 [2048, 2048], replicated, may hold values from -0.125 to 0.125
- prompt_state: float32 [8, 8, 128, 256], P('dp', 'tp', 'kv'), parts along dimension 0, may hold values from -8 to 8
- decode_state: float32 [256, 8, 128, 256], P(('dp', 'kv'), 'tp'), parts along dimension 0, may hold values from -8 to 8
Outputs:
- mixed_piece: bfloat16 [4096, 8, 2048], P(('kv', 'tp'), 'dp'), parts along dimension 1
- mixed_decode: bfloat16 [256, 2048], P(('dp', 'kv', 'tp')), parts along dimension 0
- prompt_state_out: float32 [8, 8, 128, 256], P('dp', 'tp', 'kv'), parts along dimension 0
- decode_state_out: float32 [256, 8, 128, 256], P(('dp', 'kv'), 'tp'), parts along dimension 0
There are 4 independent parts, one for each index of `dp`. A program takes and returns all parts, laid end to end along the dimension named above; an argument that names none is the same for every part. Nothing has to cross between parts.
All inputs are finite; a program needn't handle non-finite values.
Results may differ from a plain program's by a relative error of at most 0.014.
Values may be sent and summed in bfloat16 or wider, within the bound.
No kernel may reach another device: no remote copies, remote signals or barrier semaphores. Data moves between devices by JAX's collectives and lax.ppermute only.
A program may use at most 192 MiB of HBM per device.

v0:
```python
import jax
import jax.numpy as jnp
from jax import lax
from jax.sharding import PartitionSpec as P

DK = 128
DV = 256
BLOCK = 64


highest = lax.Precision.HIGHEST
norm_eps = 0.1
decay_tau = 16.0
part_limit = 16


def entering(value, axis, join, neutral):
    count, mine = (lax.axis_size(axis), lax.axis_index(axis))
    pieces = jax.tree.map(lambda part: lax.all_gather(part, axis), value)
    subtotal = jax.tree.map(
        lambda part, zero: jnp.full_like(part, 0) + jnp.asarray(zero, part.dtype), value, neutral
    )

    def step(position, subtotal):
        longer = join(subtotal, jax.tree.map(lambda part: part[position], pieces))
        return jax.tree.map(lambda new, old: jnp.where(position < mine, new, old), longer, subtotal)

    return lax.fori_loop(0, count - 1, step, subtotal)


def broadcast(block, axis, holder):
    block = jnp.where(lax.axis_index(axis) == holder, block, jnp.zeros_like(block))
    return lax.psum(block, axis)


def rms_rows(row_block, gain):
    wide = row_block.astype(jnp.float32)
    factor = lax.rsqrt(jnp.mean(wide * wide, axis=-1, keepdims=True) + norm_eps)
    return (wide * factor * gain).astype(jnp.bfloat16)


def head_norm(outputs, gain):
    factor = lax.rsqrt(jnp.mean(outputs * outputs, axis=-1, keepdims=True) + norm_eps)
    flat = (outputs * factor).reshape(outputs.shape[:-2] + (-1,))
    return (flat * gain).astype(jnp.bfloat16)


def block_terms(q_blk, k_blk, v_blk, g_blk):
    block_len = q_blk.shape[0]
    part_len = min(part_limit, block_len)
    part_count = block_len // part_len
    within = jnp.cumsum(g_blk, axis=0)
    part_ends = within[part_len - 1 :: part_len]
    anchor = jnp.concatenate([jnp.zeros_like(part_ends[:1]), part_ends[:-1]], axis=0)
    q_wide = q_blk.astype(jnp.float32)
    k_wide = k_blk.astype(jnp.float32)
    q_parts = q_wide.reshape((part_count, part_len) + q_blk.shape[1:])
    w_parts = within.reshape((part_count, part_len) + within.shape[1:])
    near_query = (q_parts * jnp.exp(w_parts - anchor[:, None])).astype(jnp.bfloat16)
    near_key = (k_wide[None] * jnp.exp(anchor[:, None] - within[None])).astype(jnp.bfloat16)
    scores = jnp.einsum(
        "itbhk,isbhk->ibhts", near_query, near_key, preferred_element_type=jnp.float32
    )
    row_pos = jnp.arange(part_count)[:, None] * part_len + jnp.arange(part_len)[None]
    keep = row_pos[:, :, None] >= jnp.arange(block_len)[None, None]
    weights = jnp.where(keep[:, None, None], scores, 0.0).astype(jnp.bfloat16)
    in_block = jnp.einsum("ibhts,sbhv->itbhv", weights, v_blk, preferred_element_type=jnp.float32)
    in_block = in_block.reshape((block_len,) + in_block.shape[2:])
    block_total = within[-1]
    start_query = (q_wide * jnp.exp(within)).astype(jnp.bfloat16)
    end_key = (k_wide * jnp.exp(block_total[None] - within)).astype(jnp.bfloat16)
    added = jnp.einsum("sbhk,sbhv->bhkv", end_key, v_blk, preferred_element_type=jnp.float32)
    return (in_block, start_query, block_total, added)


def block_form(query_all, key_all, value_all, decay_all):
    seq_len, batch_size, head_count, width_k = query_all.shape
    width_v = value_all.shape[-1]
    block_count = seq_len // BLOCK

    def to_blocks(tensor):
        return tensor.reshape((block_count, BLOCK) + tensor.shape[1:])

    def advance(carried, inputs):
        states, offset = carried
        in_block, start_query, block_total, added = block_terms(*inputs)
        new_states = jnp.exp(block_total)[..., None] * states + added
        return ((new_states, offset + block_total), (in_block, start_query, states, offset))

    start_states = jnp.zeros((batch_size, head_count, width_k, width_v), jnp.float32)
    start_log = jnp.zeros((batch_size, head_count, width_k), jnp.float32)
    (local_states, totals), (outputs, start_queries, block_starts, block_offsets) = lax.scan(
        advance,
        (start_states, start_log),
        (to_blocks(query_all), to_blocks(key_all), to_blocks(value_all), to_blocks(decay_all)),
    )
    return (outputs, start_queries, block_starts, block_offsets, local_states, totals)


def single_token(query, key_new, value_new, decay, states):
    query = query.astype(jnp.float32)
    key_new = key_new.astype(jnp.float32)
    value_new = value_new.astype(jnp.float32)
    from_state = jnp.einsum("bhk,bhkv->bhv", query * jnp.exp(decay), states, precision=highest)
    token_score = jnp.sum(query * key_new, axis=-1, keepdims=True)
    outputs = from_state + token_score * value_new
    carried = jnp.exp(decay)[..., None] * states + key_new[..., None] * value_new[..., None, :]
    return (outputs, carried)


def chain(earlier, later):
    return (earlier[0] + later[0], jnp.exp(later[0])[..., None] * earlier[1] + later[1])


def on_device(
    pieces,
    new_tokens,
    w_query,
    w_key,
    w_value,
    w_decay,
    decay_bias,
    norm_gain,
    head_gain,
    w_out,
    prompt_state,
    decode_state,
):
    tp_size = lax.axis_size("tp")
    kv_size = lax.axis_size("kv")
    tp_index = lax.axis_index("tp")
    kv_index = lax.axis_index("kv")
    heads_here = w_query.shape[1] // DK
    bias_here = lax.dynamic_slice_in_dim(decay_bias, tp_index * (heads_here * DK), heads_here * DK)
    gain_here = lax.dynamic_slice_in_dim(head_gain, tp_index * (heads_here * DV), heads_here * DV)
    own_pos, prompt_count, width = pieces.shape
    piece_count = own_pos * prompt_count
    normed_piece = rms_rows(pieces, norm_gain).reshape(piece_count, width)
    normed_dec = rms_rows(new_tokens, norm_gain)
    rows_all = jnp.concatenate([normed_piece, normed_dec], axis=0)
    row_count = rows_all.shape[0]
    row_block = lax.all_gather(rows_all, "tp", axis=0, tiled=True)
    products = jnp.concatenate(
        [
            jnp.dot(row_block, w_query, preferred_element_type=jnp.float32),
            jnp.dot(row_block, w_key, preferred_element_type=jnp.float32),
            jnp.dot(row_block, w_value, preferred_element_type=jnp.float32),
            jnp.dot(row_block, w_decay, preferred_element_type=jnp.float32),
        ],
        axis=-1,
    )
    products = products.reshape(tp_size, row_count, products.shape[-1])
    piece_prod = products[:, :piece_count].reshape(
        tp_size * own_pos, prompt_count, products.shape[-1]
    )
    dec_prod = products[:, piece_count:].reshape(
        tp_size * (row_count - piece_count), products.shape[-1]
    )

    def split_roles(product):
        lead = product.shape[:-1]
        qk_cols = heads_here * DK
        v_cols = heads_here * DV
        queries = (product[..., :qk_cols] * DK ** (-0.5)).astype(jnp.bfloat16)
        keys_new = product[..., qk_cols : 2 * qk_cols].astype(jnp.bfloat16)
        values_new = product[..., 2 * qk_cols : 2 * qk_cols + v_cols].astype(jnp.bfloat16)
        decays = jax.nn.log_sigmoid(product[..., 2 * qk_cols + v_cols :] + bias_here) / decay_tau
        return (
            queries.reshape(lead + (heads_here, DK)),
            keys_new.reshape(lead + (heads_here, DK)),
            values_new.reshape(lead + (heads_here, DV)),
            decays.reshape(lead + (heads_here, DK)),
        )

    query_p, key_p, value_p, decay_p = split_roles(piece_prod)
    in_blocks, start_queries, block_starts, block_offsets, local_states, totals = block_form(
        query_p, key_p, value_p, decay_p
    )
    whole_start = lax.all_gather(
        prompt_state.astype(jnp.bfloat16), "kv", axis=2, tiled=True
    ).astype(prompt_state.dtype)
    prefix_log, prefix_states = entering(
        (totals, local_states), "kv", chain, (jnp.zeros_like(totals), jnp.zeros_like(local_states))
    )
    incoming = jnp.exp(prefix_log)[..., None] * whole_start + prefix_states
    full_starts = block_starts + jnp.exp(block_offsets)[..., None] * incoming[None]
    from_state = jnp.einsum(
        "ntbhk,nbhkv->ntbhv", start_queries.astype(jnp.float32), full_starts, precision=highest
    )
    piece_att = (in_blocks + from_state).reshape((tp_size * own_pos,) + in_blocks.shape[2:])
    rows_k = prompt_state.shape[2]
    final_all = jnp.exp(totals)[..., None] * incoming + local_states
    final_all = broadcast(final_all.astype(jnp.bfloat16), "kv", kv_size - 1).astype(final_all.dtype)
    prompt_out = lax.dynamic_slice_in_dim(final_all, kv_index * rows_k, rows_k, 2)
    query_d, key_d, value_d, decay_d = split_roles(dec_prod)
    decode_att, decode_out = single_token(query_d, key_d, value_d, decay_d, decode_state)
    piece_normed = head_norm(piece_att, gain_here)
    dec_normed = head_norm(decode_att, gain_here)
    send_rows = jnp.concatenate(
        [
            piece_normed.reshape(tp_size, piece_count, piece_normed.shape[-1]),
            dec_normed.reshape(tp_size, dec_normed.shape[0] // tp_size, dec_normed.shape[-1]),
        ],
        axis=1,
    )
    mixed = jnp.dot(
        lax.all_to_all(send_rows, "tp", split_axis=0, concat_axis=2, tiled=True),
        w_out,
        preferred_element_type=jnp.float32,
    ).astype(jnp.bfloat16)
    mixed_piece = mixed[0, :piece_count].reshape(own_pos, prompt_count, mixed.shape[-1])
    mixed_decode = mixed[0, piece_count:]
    return (mixed_piece, mixed_decode, prompt_out, decode_out)


def solution(mesh):
    return jax.shard_map(
        on_device,
        mesh=mesh,
        in_specs=(
            P(("kv", "tp"), "dp", None),
            P(("dp", "kv", "tp"), None),
            P(None, "tp"),
            P(None, "tp"),
            P(None, "tp"),
            P(None, "tp"),
            P(),
            P(),
            P(),
            P(),
            P("dp", "tp", "kv", None),
            P(("dp", "kv"), "tp", None, None),
        ),
        out_specs=(
            P(("kv", "tp"), "dp", None),
            P(("dp", "kv", "tp"), None),
            P("dp", "tp", "kv", None),
            P(("dp", "kv"), "tp", None, None),
        ),
        check_vma=False,
    )
```

profile of v0, /device:TPU:0, one launch (start us, length us, event | category | flops | bytes accessed | tf_op | source)
XLA Modules:
  0.0 593.3 jit_solution(7355027402544248402)
XLA Ops:
  15.0 8.7 %fusion.34 = bf16[512,2,2048]{2,1,0:T(2,128)(2,1)} fusion(bf16[512,2,2048]{2,1,0:T(2,128)(2,1)} %param.16, f32[2048]{0:T(1024)S(1)} %copy-done.10, f32[512,2]{1,0:T(8,128)S(1)} %add_rsqrt_fusion), kind=kLoop, calls=%fused_computation.54 | loop fusion | flops 8388608 | bytes 8400896 | tf_op jit(solution)/shard_map/convert_element_type | solution.py:39
  36.5 22.8 %all-gather.5.cloned.1.call-done = bf16[2064,2048]{1,0:T(8,128)(2,1)} async-done(((bf16[1032,2048]{1,0:T(8,128)(2,1)}), bf16[2064,2048]{1,0:T(8,128)(2,1)}) %all-gather.5.cloned.1.call-update) | async-done | bytes 8454160 | tf_op jit(solution)/shard_map/all_gather | solution.py:142
  59.4 9.6 %fusion.61 = f32[2064,512]{1,0:T(8,128)} fusion(bf16[2064,2048]{1,0:T(8,128)(2,1)} %all-gather.5.cloned.1.call-done, bf16[2048,512]{1,0:T(8,128)(2,1)S(1)} %copy-done), kind=kOutput, calls=%fused_computation.109 | convolution fusion | flops 4328521728 | bytes 14778368 | tf_op jit(solution)/shard_map/dot_general | solution.py:148
  69.0 11.2 %fusion.60 = f32[2064,1024]{1,0:T(8,128)} fusion(bf16[2064,2048]{1,0:T(8,128)(2,1)S(1)} %copy-done.13, bf16[2048,1024]{1,0:T(8,128)(2,1)S(1)} %copy-done.14), kind=kOutput, calls=%fused_computation.108 | convolution fusion | flops 8657043456 | bytes 21102592 | tf_op jit(solution)/shard_map/dot_general | solution.py:147
  92.4 8.1 %pad_maximum_fusion = f32[2064,2560]{1,0:T(8,128)S(1)} fusion(f32[2064,512]{1,0:T(8,128)} %fusion.61, f32[2064,1024]{1,0:T(8,128)} %fusion.60, f32[2064,512]{1,0:T(8,128)} %fusion.59, f32[2064,512]{1,0:T(8,128)} %fusion.58), kind=kLoop, calls=%fused_computation.45 | loop fusion | flops 15851520 | bytes 42270720 | tf_op jit(solution)/shard_map/concatenate | solution.py:143
  107.5 7.8 %slice.66 = f32[2,1024,2560]{2,1,0:T(8,128)} slice(f32[2,1032,2560]{2,1,0:T(8,128)S(1)} %bitcast.117), slice={[0:2], [0:1024], [0:2560]} | slice | bytes 41943040 | tf_op jit(solution)/shard_map/slice | solution.py:153
  115.3 24.3 %reshape.186 = f32[1024,2,2560]{2,1,0:T(2,128)} reshape(f32[2,1024,2560]{2,1,0:T(8,128)} %slice.66) | data formatting | bytes 41943040 | tf_op jit(solution)/shard_map/reshape | solution.py:153
  139.7 9.1 %convert.14 = bf16[1024,2,2560]{2,1,0:T(2,128)(2,1)S(1)} convert(f32[1024,2,2560]{2,1,0:T(2,128)} %reshape.186) | non-fusion elementwise | flops 5242880 | bytes 31457280 | tf_op jit(solution)/shard_map/convert.9
  159.8 14.1 %fusion.40 = (bf16[1024,2,512]{2,1,0:T(2,128)(2,1)}, f32[1024,2,512]{2,1,0:T(2,128)}) fusion(f32[1024,2,2560]{2,1,0:T(2,128)} %reshape.186, f32[512]{0:T(512)S(1)} %dynamic_slice.38), kind=kLoop, calls=%fused_computation.68 | loop fusion | flops 12582912 | bytes 14682112 | tf_op jit(solution)/shard_map/convert_element_type | solution.py:164
  183.6 7.7 %reshape.204 = bf16[16,64,2,4,256]{4,3,2,1,0:T(4,128)(2,1)} reshape(bf16[1024,2,1024]{2,1,0:T(2,128)(2,1)} %slice.69) | data formatting | bytes 8388608 | tf_op jit(solution)/shard_map/reshape;reshape | solution.py:82
  194.0 145.8 %while.37 = (s32[]{:T(128)}, f32[2,4,128,256]{3,2,1,0:T(8,128)S(1)}, f32[2,4,128]{2,1,0:T(4,128)S(1)}, f32[16,64,2,4,256]{4,1,3,2,0:T(8,128)}, bf16[16,64,2,4,12...) while((s32[]{:T(128)}, ...), condition=%wide.region_4.5_spmd.clone, body=%wide.region_2.4_spmd.clone.sunk | while | flops 65543236 | bytes 11581150 | solution.py:92
  340.9 19.8 %all_gather.23 = bf16[2,4,128,256]{3,2,1,0:T(8,128)(2,1)} all-gather(bf16[2,4,32,256]{3,2,1,0:T(8,128)(2,1)S(1)} %convert_element_type.113), channel_id=1, replica_groups=mesh['dp'=4,'kv'=4,'tp'=2] {'kv'}, dimensions={2}, use_global_device_ids=true | all-gather | bytes 655360 | tf_op jit(solution)/shard_map/all_gather | solution.py:179
  369.6 13.8 %all-gather = f32[8,4,128]{2,1,0:T(4,128)S(1)} all-gather(f32[2,4,128]{2,1,0:T(4,128)S(1)} %get-tuple-element.179), channel_id=2, replica_groups=mesh['dp'=4,'kv'=4,'tp'=2] {'kv'}, dimensions={0}, use_global_device_ids=true | all-gather | bytes 20480 | tf_op jit(solution)/shard_map/all_gather | solution.py:19
  383.4 8.4 %multiply_add_fusion = f32[16,4,128,256]{3,2,1,0:T(8,128)} fusion(f32[16,4,128,256]{3,2,1,0:T(8,128)} %param.27, f32[16,4,256]{2,1,0:T(4,128)S(1)} %reshape.195, f32[16,4,128]{2,1,0:T(4,128)S(1)} %reshape.194, f32[16,4,128]{2,1,0:T(4,128)S(1)} %exp.75), kind=kLoop, calls=%fused_computation.56 | loop fusion | flops 6291456 | bytes 16908288 | tf_op jit(solution)/shard_map/add | solution.py:107
  391.7 33.7 %all-gather.7.cloned.1.call-done = f32[8,4,128,256]{3,2,1,0:T(8,128)} async-done(((f32[2,4,128,256]{3,2,1,0:T(8,128)}), f32[8,4,128,256]{3,2,1,0:T(8,128)}) %all-gather.7.cloned.1.call-update) | async-done | bytes 4194320 | tf_op jit(solution)/shard_map/all_gather | solution.py:19
  432.8 15.8 %multiply_reduce_fusion = (f32[16,64,2,4]{1,3,2,0:T(4,128)S(1)}, f32[16,64,2,4,256]{4,1,3,2,0:T(8,128)}) fusion(f32[16,64,2,4,256]{4,1,3,2,0:T(8,128)} %get-tuple-element.176, bf16[16,64,2,4,128]{4,1,3,2,0:T(8,128)(2,1)} %get-tuple-element.183, f32[16,2,4,128,256]{4,3,2,1,0:T(8,128)} %get-tuple-element.177, f32[2,4,128,256]{3,2,1,0:T(8,128)S(1)} %get-tuple-element.342, ...), kind=kOutput, calls=%fused_computation.58 | convolution fusion | flops 3235897344 | bytes 36798464 | tf_op jit(solution)/shard_map/ntbhk,nbhkv->ntbhv/dot_general | solution.py:187
  448.7 12.2 %copy.91 = f32[16,64,2,4,256]{4,3,2,1,0:T(4,128)} copy(f32[16,64,2,4,256]{4,1,3,2,0:T(8,128)} %get-tuple-element.356) | data formatting | bytes 16777216 | tf_op jit(solution)/shard_map/add | solution.py:190
  460.9 10.9 %reshape.187 = f32[2,1024,1024]{2,1,0:T(8,128)} reshape(f32[16,64,2,4,256]{4,3,2,1,0:T(4,128)} %copy.91) | data formatting | bytes 16777216 | tf_op jit(solution)/shard_map/reshape | solution.py:190
  477.0 10.7 %mul.245 = f32[2,1024,1024]{2,1,0:T(8,128)} reshape(f32[1024,2,4,256]{3,2,1,0:T(4,128)} %mul.244) | data formatting | bytes 16777216 | tf_op jit(solution)/shard_map/mul | solution.py:44
  487.8 8.1 %multiply_convert_fusion.4 = bf16[2,1024,1024]{2,1,0:T(8,128)(2,1)S(1)} fusion(f32[2,1024,1024]{2,1,0:T(8,128)} %reshape.187, f32[2,1024,1024]{2,1,0:T(8,128)} %mul.245, f32[1024]{0:T(1024)S(1)} %dynamic_slice.39), kind=kLoop, calls=%fused_computation.57 | loop fusion | flops 6291456 | bytes 20975616 | tf_op jit(solution)/shard_map/convert_element_type | solution.py:45
  503.4 40.2 %copy.94 = bf16[1,1032,2,1024]{3,2,1,0:T(2,128)(2,1)S(1)} copy(bf16[1,1032,2,1024]{3,1,2,0:T(8,128)(2,1)S(1)} %bitcast.122) | data formatting | bytes 8454144 | tf_op jit(solution)/shard_map/all_to_all | solution.py:207
  547.3 12.7 %fusion.37 = bf16[1,1032,2048]{2,1,0:T(8,128)(2,1)S(1)} fusion(bf16[1032,2048]{1,0:T(8,128)(2,1)} %bitcast.125, bf16[2048,2048]{1,0:T(8,128)(2,1)} %param.25), kind=kOutput, calls=%fused_computation.62 | convolution fusion | flops 8659156992 | bytes 16842752 | tf_op jit(solution)/shard_map/dot_general | solution.py:206
  564.3 7.6 %reshape_squeeze.3 = bf16[512,2,2048]{2,1,0:T(2,128)(2,1)} reshape(bf16[1,1024,2048]{2,1,0:T(8,128)(2,1)} %slice.76) | data formatting | bytes 8388608 | tf_op jit(solution)/shard_map/reshape;squeeze | solution.py:211
  573.3 11.6 %all-reduce.3.cloned.1.call-done = bf16[2,4,128,256]{3,2,1,0:T(8,128)(2,1)} async-done(((bf16[2,4,128,256]{3,2,1,0:T(8,128)(2,1)}), bf16[2,4,128,256]{3,2,1,0:T(8,128)(2,1)}) %all-reduce.3.cloned.1.call-update) | async-done | bytes 524304 | tf_op jit(solution)/shard_map/psum | solution.py:33
  (454 shorter events, 253.3 us)
Async XLA Ops:
  7.2 52.2 %copy-start = (bf16[2048,512]{1,0:T(8,128)(2,1)S(1)}, bf16[2048,512]{1,0:T(8,128)(2,1)}, u32[]{:S(2)}) copy-start(bf16[2048,512]{1,0:T(8,128)(2,1)} %param.21) | copy-start | bytes 6291460
  7.2 7.7 %copy-start.9 = (bf16[8,2048]{1,0:T(8,128)(2,1)S(1)}, bf16[8,2048]{1,0:T(8,128)(2,1)}, u32[]{:S(2)}) copy-start(bf16[8,2048]{1,0:T(8,128)(2,1)} %param.17) | copy-start | bytes 98308
  7.2 7.7 %copy-start.10 = (f32[2048]{0:T(1024)S(1)}, f32[2048]{0:T(1024)}, u32[]{:S(2)}) copy-start(f32[2048]{0:T(1024)} %param.23) | copy-start | bytes 24580
  7.2 52.1 %all-gather.5.cloned.1.call-start = ((), (), s32[]{:S(2)}) async-start(), calls=%async_computation.1 | async-start | bytes 12681216 | tf_op jit(solution)/shard_map/all_gather | solution.py:142
  35.8 0.7 copy-start.12
  35.8 389.7 %all-gather.7.cloned.1.call-start = ((), (), s32[]{:S(2)}) async-start(), calls=%async_computation.3 | async-start | bytes 5242880 | tf_op jit(solution)/shard_map/all_gather | solution.py:19
  59.4 9.7 %copy-start.13 = (bf16[2064,2048]{1,0:T(8,128)(2,1)S(1)}, bf16[2064,2048]{1,0:T(8,128)(2,1)}, u32[]{:S(2)}) copy-start(bf16[2064,2048]{1,0:T(8,128)(2,1)} %all-gather.5.cloned.1.call-done) | copy-start | bytes 25362436
  59.4 9.7 %copy-start.14 = (bf16[2048,1024]{1,0:T(8,128)(2,1)S(1)}, bf16[2048,1024]{1,0:T(8,128)(2,1)}, u32[]{:S(2)}) copy-start(bf16[2048,1024]{1,0:T(8,128)(2,1)} %param.20) | copy-start | bytes 12582916
  69.0 11.2 %copy-start.15 = (bf16[2048,512]{1,0:T(8,128)(2,1)S(1)}, bf16[2048,512]{1,0:T(8,128)(2,1)}, u32[]{:S(2)}) copy-start(bf16[2048,512]{1,0:T(8,128)(2,1)} %param.19) | copy-start | bytes 6291460
  80.2 6.1 %copy-start.16 = (bf16[2048,512]{1,0:T(8,128)(2,1)S(1)}, bf16[2048,512]{1,0:T(8,128)(2,1)}, u32[]{:S(2)}) copy-start(bf16[2048,512]{1,0:T(8,128)(2,1)} %param.18) | copy-start | bytes 6291460
  100.5 7.1 %copy-start.4 = (f32[2064,2560]{1,0:T(8,128)}, f32[2064,2560]{1,0:T(8,128)S(1)}, u32[]{:S(2)}) copy-start(f32[2064,2560]{1,0:T(8,128)S(1)} %pad_maximum_fusion) | copy-start | bytes 63406084
  148.8 4.0 copy-start.5
  173.9 7.1 %slice-start = ((bf16[1024,2,2560]{2,1,0:T(2,128)(2,1)}), bf16[1024,2,512]{2,1,0:T(2,128)(2,1)S(1)}, s32[]{:S(2)}) async-start(bf16[1024,2,2560]{2,1,0:T(2,128)(2,1)} %copy-done.5), calls=%async_computation.4 | async-start | bytes 4194304 | tf_op jit(solution)/shard_map/slice | solution.py:165
  183.6 7.7 %copy-start.6 = (bf16[1024,2,512]{2,1,0:T(2,128)(2,1)S(1)}, bf16[1024,2,512]{2,1,0:T(2,128)(2,1)}, u32[]{:S(2)}) copy-start(bf16[1024,2,512]{2,1,0:T(2,128)(2,1)} %get-tuple-element.349) | copy-start | bytes 6291460
  193.9 146.9 %copy-start.8 = (f32[2,4,32,256]{3,2,1,0:T(8,128)S(1)}, f32[2,4,32,256]{3,2,1,0:T(8,128)}, u32[]{:S(2)}) copy-start(f32[2,4,32,256]{3,2,1,0:T(8,128)} %param.26) | copy-start | bytes 786436
  193.9 146.9 %copy-start.11 = (f32[2048]{0:T(1024)S(1)}, f32[2048]{0:T(1024)}, u32[]{:S(2)}) copy-start(f32[2048]{0:T(1024)} %param.24) | copy-start | bytes 24580
  339.7 1.0 copy-start.2
  340.7 244.2 %all-reduce.3.cloned.1.call-start = ((), (), s32[]{:S(2)}) async-start(), calls=%async_computation.2 | async-start | bytes 1048576 | tf_op jit(solution)/shard_map/psum | solution.py:33
  425.5 5.1 copy-start.3
  560.0 2.0 copy-start.7
  562.0 24.6 %copy-start.1 = (bf16[2048,512]{1,0:T(8,128)(2,1)S(1)}, bf16[2048,512]{1,0:T(8,128)(2,1)}, u32[]{:S(2)}) copy-start(bf16[2048,512]{1,0:T(8,128)(2,1)} %param.21) | copy-start | bytes 6291460
Sparse Core Ops, SparseCore 0:
  35.9 23.3 all-gather.4
  340.8 84.5 all-gather.6
  547.5 37.4 all-reduce.2
where the time goes:
time: 604 us; the launch traced here: 593 us
  local copies, waits for them, and re-layouts  220 us (36%)
  other arithmetic  163 us (27%)
  matrix products  85 us (14%)
  waiting for transfers between devices  68.3 us (11%)
  blocking collectives  40.7 us (7%)
  between operations  14.3 us (2%)
    all_to_all x1, local copies, waits for them, and re-layouts, on_device(): lax.all_to_all(send_rows, 'tp', split_axis=0, concat_axis=2, tiled=True)  40.2 us
    all_gather x1, waiting for transfers between devices, entering(): pieces = jax.tree.map(lambda part: lax.all_gather(part, axis), value)  33.7 us
    reshape x1, local copies, waits for them, and re-layouts, on_device(): products[:, :piece_count]  24.3 us
    dynamic_update_slice x32, local copies, waits for them, and re-layouts, block_form(): lax.scan(advance, (start_states, start_log), (to_blocks(query_all), to_bl...  24.2 us
    all_gather x1, waiting for transfers between devices, on_device(): row_block = lax.all_gather(rows_all, 'tp', axis=0, tiled=True)  22.8 us
    another operation x4, local copies, waits for them, and re-layouts, to_blocks(): return tensor.reshape((block_count, BLOCK) + tensor.shape[1:])  20.1 us
    all_gather x1, blocking collectives, on_device(): lax.all_gather(prompt_state.astype(jnp.bfloat16), 'kv', axis=2, tiled=True)  19.8 us
    dynamic_update_slice x32, other arithmetic, block_form(): lax.scan(advance, (start_states, start_log), (to_blocks(query_all), to_bl...  17.8 us
  transfers between devices with their start and end apart: 3, of which 3 were waited for; matrix products, arithmetic and copies ran while one was open for 7% of the time, Pallas kernels for 0%

commit v1 on v0

v1 whole, which is shorter than its diff:
```python
import jax
import jax.numpy as jnp
from jax import lax
from jax.experimental import pallas as pl
from jax.experimental.pallas import tpu as pltpu
from jax.sharding import PartitionSpec as P

DK = 128
DV = 256
BLOCK = 64


highest = lax.Precision.HIGHEST
norm_eps = 0.1
decay_tau = 16.0
part_limit = 16


def rms_rows(row_block, gain):
    wide = row_block.astype(jnp.float32)
    factor = lax.rsqrt(jnp.mean(wide * wide, axis=-1, keepdims=True) + norm_eps)
    return (wide * factor * gain).astype(jnp.bfloat16)


def head_norm(outputs, gain):
    factor = lax.rsqrt(jnp.mean(outputs * outputs, axis=-1, keepdims=True) + norm_eps)
    flat = (outputs * factor).reshape(outputs.shape[:-2] + (-1,))
    return (flat * gain).astype(jnp.bfloat16)


def single_token(query, key_new, value_new, decay, states):
    query = query.astype(jnp.float32)
    key_new = key_new.astype(jnp.float32)
    value_new = value_new.astype(jnp.float32)
    from_state = jnp.einsum("bhk,bhkv->bhv", query * jnp.exp(decay), states, precision=highest)
    token_score = jnp.sum(query * key_new, axis=-1, keepdims=True)
    outputs = from_state + token_score * value_new
    carried = jnp.exp(decay)[..., None] * states + key_new[..., None] * value_new[..., None, :]
    return (outputs, carried)


NT = (((1,), (1,)), ((), ()))
TN = (((0,), (0,)), ((), ()))


def split_sum(selector, wide):
    high = wide.astype(jnp.bfloat16)
    rest = wide - high.astype(jnp.float32)
    middle = rest.astype(jnp.bfloat16)
    low = (rest - middle.astype(jnp.float32)).astype(jnp.bfloat16)
    dot = lambda part: jnp.dot(selector, part, preferred_element_type=jnp.float32)
    return dot(high) + (dot(middle) + dot(low))


def as_column(row):
    return jnp.transpose(jnp.broadcast_to(row, (8, row.shape[1])))[:, :1]


def positions(shape, axis):
    return lax.broadcasted_iota(jnp.int32, shape, axis)


def local_state_kernel(k_ref, v_ref, g_ref, state_ref, total_ref):
    rows = k_ref.shape[1]
    heads = k_ref.shape[2] // DK

    @pl.when(pl.program_id(1) == 0)
    def _():
        state_ref[...] = jnp.zeros_like(state_ref)
        total_ref[...] = jnp.zeros_like(total_ref)

    decay = g_ref[0]
    later = (positions((rows, rows), 1) > positions((rows, rows), 0)).astype(jnp.bfloat16)
    after = split_sum(later, decay)
    total = after[:1] + decay[:1]
    end_key = (k_ref[0].astype(jnp.float32) * jnp.exp(after)).astype(jnp.bfloat16)
    for head in range(heads):
        ks = slice(head * DK, (head + 1) * DK)
        vs = slice(head * DV, (head + 1) * DV)
        added = lax.dot_general(
            end_key[:, ks], v_ref[0, :, vs], TN, preferred_element_type=jnp.float32
        )
        state_ref[0, head] = as_column(jnp.exp(total[:, ks])) * state_ref[0, head] + added
    total_ref[0] = total_ref[0] + total


def attention_kernel(q_ref, k_ref, v_ref, g_ref, start_ref, gain_ref, out_ref, state_ref):
    rows = q_ref.shape[1]
    heads = q_ref.shape[2] // DK
    parts = BLOCK // part_limit

    @pl.when(pl.program_id(1) == 0)
    def _():
        state_ref[...] = start_ref[0]

    t_pos = positions((rows, rows), 0)
    s_pos = positions((rows, rows), 1)
    same_part = (t_pos // part_limit == s_pos // part_limit) & (s_pos <= t_pos)
    near_all = split_sum(same_part.astype(jnp.bfloat16), g_ref[0])
    row_t = positions((BLOCK, parts * BLOCK), 0)
    col = positions((BLOCK, parts * BLOCK), 1)
    keep = (row_t // part_limit == col // BLOCK) & (col % BLOCK <= row_t)
    for block in range(rows // BLOCK):
        at = slice(block * BLOCK, (block + 1) * BLOCK)
        near = near_all[at]
        q_wide = q_ref[0, at].astype(jnp.float32)
        k_wide = k_ref[0, at].astype(jnp.float32)
        v_blk = v_ref[0, at]
        anchors = [jnp.zeros_like(near[:1])]
        for part in range(parts):
            last = (part + 1) * part_limit - 1
            anchors.append(anchors[-1] + near[last : last + 1])
        total = anchors[-1]
        within = jnp.concatenate(
            [
                near[part * part_limit : (part + 1) * part_limit] + anchors[part]
                for part in range(parts)
            ],
            axis=0,
        )
        near_query = (q_wide * jnp.exp(near)).astype(jnp.bfloat16)
        near_key = jnp.concatenate(
            [k_wide * jnp.exp(anchors[part] - within) for part in range(parts)], axis=0
        ).astype(jnp.bfloat16)
        start_query = (q_wide * jnp.exp(within)).astype(jnp.bfloat16)
        end_key = (k_wide * jnp.exp(total - within)).astype(jnp.bfloat16)
        kept = jnp.exp(total)
        for head in range(heads):
            ks = slice(head * DK, (head + 1) * DK)
            vs = slice(head * DV, (head + 1) * DV)
            v_head = v_blk[:, vs]
            scores = lax.dot_general(
                near_query[:, ks], near_key[:, ks], NT, preferred_element_type=jnp.float32
            )
            weights = jnp.where(keep, scores, 0.0).astype(jnp.bfloat16)
            state = state_ref[head]
            att = jnp.dot(
                weights,
                jnp.concatenate([v_head] * parts, axis=0),
                preferred_element_type=jnp.float32,
            ) + jnp.dot(
                start_query[:, ks], state.astype(jnp.bfloat16), preferred_element_type=jnp.float32
            )
            added = lax.dot_general(end_key[:, ks], v_head, TN, preferred_element_type=jnp.float32)
            state_ref[head] = as_column(kept[:, ks]) * state + added
            factor = lax.rsqrt(jnp.mean(att * att, axis=-1, keepdims=True) + norm_eps)
            out_ref[0, at, vs] = (att * factor * gain_ref[:, vs]).astype(jnp.bfloat16)


def hand_on(values, axis):
    count = lax.axis_size(axis)
    return lax.ppermute(values, axis, [(at, at + 1) for at in range(count - 1)])


def on_device(
    pieces,
    new_tokens,
    w_query,
    w_key,
    w_value,
    w_decay,
    decay_bias,
    norm_gain,
    head_gain,
    w_out,
    prompt_state,
    decode_state,
):
    tp_size = lax.axis_size("tp")
    kv_size = lax.axis_size("kv")
    tp_index = lax.axis_index("tp")
    kv_index = lax.axis_index("kv")
    heads = w_query.shape[1] // DK
    bias_here = lax.dynamic_slice_in_dim(decay_bias, tp_index * (heads * DK), heads * DK)
    gain_here = lax.dynamic_slice_in_dim(head_gain, tp_index * (heads * DV), heads * DV)
    own_pos, prompt_count, width = pieces.shape
    piece_count = own_pos * prompt_count
    whole_start = lax.all_gather(prompt_state.astype(jnp.bfloat16), "kv", axis=2, tiled=True)
    normed_piece = rms_rows(pieces, norm_gain).transpose(1, 0, 2).reshape(piece_count, width)
    rows_all = jnp.concatenate([normed_piece, rms_rows(new_tokens, norm_gain)], axis=0)
    row_count = rows_all.shape[0]
    dec_count = row_count - piece_count
    row_block = lax.all_gather(rows_all, "tp", axis=0, tiled=True)

    def project(weight):
        return jnp.dot(row_block, weight, preferred_element_type=jnp.float32)

    by_owner = lambda value: value.reshape(tp_size, row_count, value.shape[-1])
    keys = by_owner(project(w_key).astype(jnp.bfloat16))
    values = by_owner(project(w_value).astype(jnp.bfloat16))
    decays = by_owner(jax.nn.log_sigmoid(project(w_decay) + bias_here) / decay_tau)
    queries = by_owner((project(w_query) * DK ** (-0.5)).astype(jnp.bfloat16))

    def row_spec(step, columns):
        per_owner = own_pos // step

        def where(prompt, at):
            return (at // per_owner, prompt * per_owner + at % per_owner, 0)

        return pl.BlockSpec((1, step, columns), where)

    step = 2 * BLOCK if own_pos % (2 * BLOCK) == 0 else BLOCK
    steps = tp_size * own_pos // step
    order = pltpu.CompilerParams(dimension_semantics=("arbitrary", "arbitrary"))
    state_spec = pl.BlockSpec((1, heads, DK, DV), lambda prompt, at: (prompt, 0, 0, 0))
    local_states, totals = pl.pallas_call(
        local_state_kernel,
        grid=(prompt_count, steps),
        in_specs=[row_spec(step, heads * DK), row_spec(step, heads * DV), row_spec(step, heads * DK)],
        out_specs=[state_spec, pl.BlockSpec((1, 1, heads * DK), lambda prompt, at: (prompt, 0, 0))],
        out_shape=[
            jax.ShapeDtypeStruct((prompt_count, heads, DK, DV), jnp.float32),
            jax.ShapeDtypeStruct((prompt_count, 1, heads * DK), jnp.float32),
        ],
        compiler_params=order,
        name="local_state",
    )(keys, values, decays)
    kept = jnp.exp(totals).reshape(prompt_count, heads, DK)[..., None]
    incoming = [whole_start[at].astype(jnp.float32) for at in range(prompt_count)]
    for hop in range(kv_size - 1):
        for at in range(prompt_count):
            leaving = (kept[at] * incoming[at] + local_states[at]).astype(jnp.bfloat16)
            arrived = hand_on(leaving, "kv").astype(jnp.float32)
            incoming[at] = jnp.where(kv_index == hop + 1, arrived, incoming[at])
    incoming = jnp.stack(incoming)
    send_rows = pl.pallas_call(
        attention_kernel,
        grid=(prompt_count, steps),
        in_specs=[
            row_spec(step, heads * DK),
            row_spec(step, heads * DK),
            row_spec(step, heads * DV),
            row_spec(step, heads * DK),
            state_spec,
            pl.BlockSpec((1, heads * DV), lambda prompt, at: (0, 0)),
        ],
        out_specs=row_spec(step, heads * DV),
        out_shape=jax.ShapeDtypeStruct((tp_size, row_count, heads * DV), jnp.bfloat16),
        scratch_shapes=[pltpu.VMEM((heads, DK, DV), jnp.float32)],
        compiler_params=order,
        name="attention",
    )(queries, keys, values, decays, incoming, gain_here[None])
    final_all = (kept * incoming + local_states).astype(jnp.bfloat16)
    rows_k = prompt_state.shape[2]
    last = kv_size - 1
    slices = [final_all[:, :, at * rows_k : (at + 1) * rows_k] for at in range(kv_size)]
    prompt_out = slices[last]
    for at in range(last):
        arrived = lax.ppermute(slices[at], "kv", [(last, at)])
        prompt_out = jnp.where(kv_index == at, arrived, prompt_out)
    prompt_out = prompt_out.astype(jnp.float32)

    def decode_rows(value, columns):
        picked = value[:, piece_count:].reshape(tp_size * dec_count, heads, columns)
        return picked

    decode_att, decode_out = single_token(
        decode_rows(queries, DK),
        decode_rows(keys, DK),
        decode_rows(values, DV),
        decode_rows(decays, DK),
        decode_state,
    )
    dec_normed = head_norm(decode_att, gain_here).reshape(tp_size, dec_count, heads * DV)
    send_rows = lax.dynamic_update_slice(send_rows, dec_normed, (0, piece_count, 0))
    mixed = jnp.dot(
        lax.all_to_all(send_rows, "tp", split_axis=0, concat_axis=2, tiled=True)[0],
        w_out,
        preferred_element_type=jnp.float32,
    ).astype(jnp.bfloat16)
    mixed_piece = mixed[:piece_count].reshape(prompt_count, own_pos, width).transpose(1, 0, 2)
    return (mixed_piece, mixed[piece_count:], prompt_out, decode_out)


def solution(mesh):
    return jax.shard_map(
        on_device,
        mesh=mesh,
        in_specs=(
            P(("kv", "tp"), "dp", None),
            P(("dp", "kv", "tp"), None),
            P(None, "tp"),
            P(None, "tp"),
            P(None, "tp"),
            P(None, "tp"),
            P(),
            P(),
            P(),
            P(),
            P("dp", "tp", "kv", None),
            P(("dp", "kv"), "tp", None, None),
        ),
        out_specs=(
            P(("kv", "tp"), "dp", None),
            P(("dp", "kv", "tp"), None),
            P("dp", "tp", "kv", None),
            P(("dp", "kv"), "tp", None, None),
        ),
        check_vma=False,
    )
```

time: 604 us -> 251 us (0.42); the launches traced: 593 us -> 248 us
  local copies, waits for them, and re-layouts: 220 us -> 55.9 us
  other arithmetic: 163 us -> 27.3 us
  waiting for transfers between devices: 68.3 us -> 14.3 us
  Pallas kernels: 0 us -> 38.1 us
  matrix products: 85 us -> 49.2 us
  starting transfers between devices: 0.59 us -> 22.8 us
  blocking collectives: 40.7 us -> 26.1 us
    convert_element_type x52 -> x6, other arithmetic: 69.9 us -> 5.5 us  [the longest x3 2.56 us: on_device(): leaving = (kept[at] * incoming[at] + local_states[at]).astype(jnp.bfloat16)]
    pallas_call x0 -> x2, Pallas kernels: none -> 38.1 us  [the longest x1 22.3 us: on_device(): pl.pallas_call(attention_kernel, grid=(prompt_count, steps), in_specs=[ro...]
    reshape x4 -> x1, local copies, waits for them, and re-layouts: 43.4 us -> 6.32 us  [on_device(): mixed[:piece_count].reshape(prompt_count, own_pos, width).transpose(1, 0, 2)]
    all_gather x1 -> x0, waiting for transfers between devices: 33.7 us -> none  [entering(): pieces = jax.tree.map(lambda part: lax.all_gather(part, axis), value)]
    dot_general x37 -> x4, matrix products: 66 us -> 33.6 us  [project(): return jnp.dot(row_block, weight, preferred_element_type=jnp.float32)]
    another operation x22 -> x0, local copies, waits for them, and re-layouts: 29.5 us -> none  [the longest x4 20.1 us: to_blocks(): return tensor.reshape((block_count, BLOCK) + tensor.shape[1:])]
    another operation x17 -> x1, other arithmetic: 26.7 us -> 1.19 us  [on_device(): incoming = jnp.stack(incoming)]
    dynamic_update_slice x32 -> x0, local copies, waits for them, and re-layouts: 24.2 us -> none  [block_form(): lax.scan(advance, (start_states, start_log), (to_blocks(query_all), to_bl...]
  transfers between devices with their start and end apart: 3 -> 10, of which waited for: 3 -> 4; matrix products, arithmetic and copies ran while one was open for 7% -> 16% of each run, Pallas kernels for 0% -> 0%
where the time goes in v1:
time: 251 us; the launch traced here: 248 us
  local copies, waits for them, and re-layouts  55.9 us (22%)
  matrix products  49.2 us (20%)
  Pallas kernels  38.1 us (15%)
  other arithmetic  27.3 us (11%)
  blocking collectives  26.1 us (10%)
  starting transfers between devices  22.8 us (9%)
  between operations  14.5 us (6%)
  waiting for transfers between devices  14.3 us (6%)
    all_to_all x1, local copies, waits for them, and re-layouts, on_device(): lax.all_to_all(send_rows, 'tp', split_axis=0, concat_axis=2, tiled=True)[0]  40.2 us
    dot_general x4, matrix products, project(): return jnp.dot(row_block, weight, preferred_element_type=jnp.float32)  33.6 us
    pallas_call x1, Pallas kernels, on_device(): pl.pallas_call(attention_kernel, grid=(prompt_count, steps), in_specs=[ro...  22.3 us
    ppermute x6, starting transfers between devices, hand_on(): return lax.ppermute(values, axis, [(at, at + 1) for at in range(count - 1)])  19.9 us
    all_gather x1, blocking collectives, on_device(): lax.all_gather(prompt_state.astype(jnp.bfloat16), 'kv', axis=2, tiled=True)  17.5 us
    pallas_call x1, Pallas kernels, on_device(): pl.pallas_call(local_state_kernel, grid=(prompt_count, steps), in_specs=[...  15.8 us
    ppermute x6, waiting for transfers between devices, hand_on(): return lax.ppermute(values, axis, [(at, at + 1) for at in range(count - 1)])  9.91 us
    dot_general x1, matrix products, on_device(): jnp.dot(lax.all_to_all(send_rows, 'tp', split_axis=0, concat_axis=2, tile...  9.24 us
  transfers between devices with their start and end apart: 10, of which 4 were waited for; matrix products, arithmetic and copies ran while one was open for 16% of the time, Pallas kernels for 0%

profile of v1, /device:TPU:0, one launch (start us, length us, event | category | flops | bytes accessed | tf_op | source)
XLA Modules:
  0.0 248.2 jit_solution(14914691937747086668)
XLA Ops:
  8.3 4.8 %fusion = f32[512,2]{0,1:T(2,128)S(1)} fusion(bf16[512,2,2048]{2,1,0:T(2,128)(2,1)} %param.12), kind=kLoop, calls=%fused_computation.3 | loop fusion | flops 6290432 | bytes 4198400 | tf_op jit(solution)/shard_map/reduce_sum | solution.py:21
  13.2 2.5 %fusion.2 = bf16[512,2,2048]{2,0,1:T(8,128)(2,1)S(1)} fusion(f32[2048]{0:T(1024)S(1)} %copy-done.11, f32[512,2]{0,1:T(2,128)S(1)} %add_rsqrt_fusion.1, bf16[512,2,2048]{2,1,0:T(2,128)(2,1)S(1)} %copy-done.4), kind=kLoop, calls=%fused_computation.5 | loop fusion | flops 8388608 | bytes 8400896 | tf_op jit(solution)/shard_map/convert_element_type | solution.py:22
  19.7 17.5 %all_gather.7 = bf16[2,4,128,256]{3,2,1,0:T(8,128)(2,1)S(1)} all-gather(bf16[2,4,32,256]{3,2,1,0:T(8,128)(2,1)S(1)} %convert_element_type.118), channel_id=1, replica_groups=mesh['dp'=4,'kv'=4,'tp'=2] {'kv'}, dimensions={2}, use_global_device_ids=true | all-gather | bytes 655360 | tf_op jit(solution)/shard_map/all_gather | solution.py:178
  37.3 4.4 %all-gather.2.cloned.1.call-done = bf16[2064,2048]{1,0:T(8,128)(2,1)} async-done(((bf16[1032,2048]{1,0:T(8,128)(2,1)}), bf16[2064,2048]{1,0:T(8,128)(2,1)}) %all-gather.2.cloned.1.call-update) | async-done | bytes 8454160 | tf_op jit(solution)/shard_map/all_gather | solution.py:183
  41.7 12.8 %convolution_convert_fusion.1 = bf16[2064,1024]{1,0:T(8,128)(2,1)S(1)} fusion(bf16[2064,2048]{1,0:T(8,128)(2,1)} %all-gather.2.cloned.1.call-done, bf16[2048,1024]{1,0:T(8,128)(2,1)} %param.16), kind=kOutput, calls=%fused_computation.8 | convolution fusion | flops 8659156992 | bytes 16875520 | tf_op jit(solution)/shard_map/dot_general | solution.py:186
  54.5 6.8 %fusion.6 = f32[2064,512]{1,0:T(8,128)S(1)} fusion(bf16[2064,2048]{1,0:T(8,128)(2,1)S(1)} %copy-done.14, bf16[2048,512]{1,0:T(8,128)(2,1)S(1)} %copy-done, f32[512]{0:T(512)S(1)} %dynamic_slice.6), kind=kOutput, calls=%fused_computation.15 | convolution fusion | flops 4339089408 | bytes 14780416 | tf_op jit(solution)/shard_map/dot_general | solution.py:186
  63.3 5.7 %convolution_convert_fusion.2 = bf16[2064,512]{1,0:T(8,128)(2,1)} fusion(bf16[2064,2048]{1,0:T(8,128)(2,1)S(1)} %copy-done.14, bf16[2048,512]{1,0:T(8,128)(2,1)S(1)} %copy-done.15), kind=kOutput, calls=%fused_computation.13 | convolution fusion | flops 4329578496 | bytes 12664832 | tf_op jit(solution)/shard_map/dot_general | solution.py:186
  69.0 15.8 %local_state.1 = (f32[2,4,128,256]{3,2,1,0:T(8,128)}, f32[2,1,512]{2,1,0:T(1,128)}) custom-call(bf16[2,1032,512]{2,1,0:T(8,128)(2,1)} %bitcast.94, bf16[2,1032,1024]{2,1,0:T(8,128)(2,1)} %bitcast.85, f32[2,1032,512]{2,1,0:T(8,128)} %bitcast.88), custom_call_target="tpu_custom_call" | custom-call | tf_op jit(solution)/shard_map/local_state/pallas_call | solution.py:206
  87.7 3.7 %collective-permute-start = (bf16[4,128,256]{2,1,0:T(8,128)(2,1)S(1)}, bf16[4,128,256]{2,1,0:T(8,128)(2,1)S(1)}, u32[]{:S(2)}, u32[]{:S(2)}) collective-permute-start(bf16[4,128,256]{2,1,0:T(8,128)(2,1)S(1)} %get-tuple-element.12), channel_id=1, source_target_pairs={{0,2},{2,4},{4,6},{1,3},{3,5},{5,7},{8,10},{10,12},{12,14},{9,11},... | collective-permute-start | bytes 786440 | tf_op jit(solution)/shard_map/ppermute | solution.py:152
  91.3 3.6 %collective-permute-start.3 = (bf16[4,128,256]{2,1,0:T(8,128)(2,1)S(1)}, bf16[4,128,256]{2,1,0:T(8,128)(2,1)S(1)}, u32[]{:S(2)}, u32[]{:S(2)}) collective-permute-start(bf16[4,128,256]{2,1,0:T(8,128)(2,1)S(1)} %get-tuple-element.13), channel_id=1, source_target_pairs={{0,2},{2,4},{4,6},{1,3},{3,5},{5,7},{8,10},{10,12},{12,14},{9,11},... | collective-permute-start | bytes 786440 | tf_op jit(solution)/shard_map/ppermute | solution.py:152
  95.1 8.1 %multiply_add_fusion = f32[16,4,128,256]{3,2,1,0:T(8,128)} fusion(f32[16,4,128,256]{3,2,1,0:T(8,128)} %param.23, f32[16,4,256]{2,1,0:T(4,128)S(1)} %reshape.114, f32[16,4,128]{2,1,0:T(4,128)S(1)} %reshape.113, f32[16,4,128]{2,1,0:T(4,128)S(1)} %exp.22), kind=kLoop, calls=%fused_computation.6 | loop fusion | flops 6291456 | bytes 16908288 | tf_op jit(solution)/shard_map/add | solution.py:38
  103.2 8.3 %fusion.4 = bf16[2064,512]{1,0:T(8,128)(2,1)S(1)} fusion(bf16[2064,2048]{1,0:T(8,128)(2,1)} %all-gather.2.cloned.1.call-done, bf16[2048,512]{1,0:T(8,128)(2,1)S(1)} %copy-done.16), kind=kOutput, calls=%fused_computation.12 | convolution fusion | flops 4330635264 | bytes 12664832 | tf_op jit(solution)/shard_map/dot_general | solution.py:186
  113.1 3.4 %collective-permute-start.1 = (bf16[4,128,256]{2,1,0:T(8,128)(2,1)S(1)}, bf16[4,128,256]{2,1,0:T(8,128)(2,1)S(1)}, u32[]{:S(2)}, u32[]{:S(2)}) collective-permute-start(bf16[4,128,256]{2,1,0:T(8,128)(2,1)S(1)} %get-tuple-element.10), channel_id=1, source_target_pairs={{0,2},{2,4},{4,6},{1,3},{3,5},{5,7},{8,10},{10,12},{12,14},{9,11},... | collective-permute-start | bytes 786440 | tf_op jit(solution)/shard_map/ppermute | solution.py:152
  118.5 6.4 %fusion.25 = f32[16,4,1,256]{3,2,1,0:T(1,128)S(1)} fusion(f32[16,4,128,1]{2,3,1,0:T(1,128)S(1)} %bitcast.101, f32[16,4,128,256]{3,2,1,0:T(8,128)} %param.23), kind=kOutput, calls=%fused_computation.67 | convolution fusion | flops 25165824 | bytes 8486912 | tf_op jit(solution)/shard_map/bhk,bhkv->bhv/dot_general | solution.py:35
  125.0 2.6 %collective-permute-done.4 = bf16[4,128,256]{2,1,0:T(8,128)(2,1)S(1)} collective-permute-done((bf16[4,128,256]{2,1,0:T(8,128)(2,1)S(1)}, bf16[4,128,256]{2,1,0:T(8,128)(2,1)S(1)}, u32[]{:S(2)}, u32[]{:S(2)}) %collective-permute-start.4) | collective-permute-done | bytes 262176 | tf_op jit(solution)/shard_map/ppermute | solution.py:152
  128.5 4.4 %collective-permute-start.2 = (bf16[4,128,256]{2,1,0:T(8,128)(2,1)}, bf16[4,128,256]{2,1,0:T(8,128)(2,1)S(1)}, u32[]{:S(2)}, u32[]{:S(2)}) collective-permute-start(bf16[4,128,256]{2,1,0:T(8,128)(2,1)} %get-tuple-element.8), channel_id=1, source_target_pairs={{0,2},{2,4},{4,6},{1,3},{3,5},{5,7},{8,10},{10,12},{12,14},{9,11},... | collective-permute-start | bytes 786440 | tf_op jit(solution)/shard_map/ppermute | solution.py:152
  132.9 2.9 %collective-permute-start.5 = (bf16[4,128,256]{2,1,0:T(8,128)(2,1)S(1)}, bf16[4,128,256]{2,1,0:T(8,128)(2,1)}, u32[]{:S(2)}, u32[]{:S(2)}) collective-permute-start(bf16[4,128,256]{2,1,0:T(8,128)(2,1)S(1)} %get-tuple-element.9), channel_id=1, source_target_pairs={{0,2},{2,4},{4,6},{1,3},{3,5},{5,7},{8,10},{10,12},{12,14},{9,11},... | collective-permute-start | bytes 786440 | tf_op jit(solution)/shard_map/ppermute | solution.py:152
  136.0 3.9 %collective-permute-done.2 = bf16[4,128,256]{2,1,0:T(8,128)(2,1)S(1)} collective-permute-done((bf16[4,128,256]{2,1,0:T(8,128)(2,1)}, bf16[4,128,256]{2,1,0:T(8,128)(2,1)S(1)}, u32[]{:S(2)}, u32[]{:S(2)}) %collective-permute-start.2) | collective-permute-done | bytes 262176 | tf_op jit(solution)/shard_map/ppermute | solution.py:152
  139.9 3.4 %collective-permute-done.5 = bf16[4,128,256]{2,1,0:T(8,128)(2,1)} collective-permute-done((bf16[4,128,256]{2,1,0:T(8,128)(2,1)S(1)}, bf16[4,128,256]{2,1,0:T(8,128)(2,1)}, u32[]{:S(2)}, u32[]{:S(2)}) %collective-permute-start.5) | collective-permute-done | bytes 262176 | tf_op jit(solution)/shard_map/ppermute | solution.py:152
  145.7 22.3 %attention.1 = bf16[2,1032,1024]{2,1,0:T(8,128)(2,1)} custom-call(bf16[2,1032,512]{2,1,0:T(8,128)(2,1)} %bitcast.100, bf16[2,1032,512]{2,1,0:T(8,128)(2,1)} %bitcast.96, bf16[2,1032,1024]{2,1,0:T(8,128)(2,1)} %bitcast.86, f32[2,1032,512]{2,1,0:T(8,128)} %bitcast.89, f32[2,4,128,256]{3,2,1,0:T(8,128)} %get-tuple-element.15.start_ref, f32[1,1024]{1,0:T(1,128)} %bitcast.102), custom_call_target="tpu_custom_call" | custom-call | tf_op jit(solution)/shard_map/attention/pallas_call | solution.py:226
  168.7 8.5 %all_to_all.15 = bf16[2,1032,1024]{2,1,0:T(8,128)(2,1)S(1)} all-to-all(bf16[2,1032,1024]{2,1,0:T(8,128)(2,1)} %fusion.21), channel_id=1, replica_groups=mesh['dp'=4,'kv'=4,'tp'=2] {'tp'}, dimensions={0} | all-to-all | bytes 8454144 | tf_op jit(solution)/shard_map/all_to_all | solution.py:267
  177.2 40.2 %copy.18 = bf16[1,1032,2,1024]{3,2,1,0:T(2,128)(2,1)S(1)} copy(bf16[1,1032,2,1024]{3,1,2,0:T(8,128)(2,1)S(1)} %bitcast.90) | data formatting | bytes 8454144 | tf_op jit(solution)/shard_map/all_to_all | solution.py:267
  222.8 9.2 %convolution_convert_fusion = bf16[1032,2048]{1,0:T(8,128)(2,1)S(1)} fusion(bf16[1032,2048]{1,0:T(8,128)(2,1)S(1)} %bitcast.97, bf16[2048,2048]{1,0:T(8,128)(2,1)S(1)} %bitcast.111), kind=kOutput, calls=%fused_computation.7 | convolution fusion | flops 8659156992 | bytes 16842752 | tf_op jit(solution)/shard_map/dot_general | solution.py:266
  233.3 6.3 %copy.31 = bf16[2,512,2048]{2,0,1:T(2,128)(2,1)} copy(bf16[2,512,2048]{2,1,0:T(8,128)(2,1)S(1)} %bitcast.93) | data formatting | bytes 8388608 | tf_op jit(solution)/shard_map/reshape | solution.py:271
  (85 shorter events, 26.2 us)
Async XLA Ops:
  7.2 47.3 %copy-start = (bf16[2048,512]{1,0:T(8,128)(2,1)S(1)}, bf16[2048,512]{1,0:T(8,128)(2,1)}, u32[]{:S(2)}) copy-start(bf16[2048,512]{1,0:T(8,128)(2,1)} %param.17) | copy-start | bytes 6291460
  7.2 5.9 %copy-start.9 = (bf16[8,2048]{1,0:T(8,128)(2,1)S(1)}, bf16[8,2048]{1,0:T(8,128)(2,1)}, u32[]{:S(2)}) copy-start(bf16[8,2048]{1,0:T(8,128)(2,1)} %param.13) | copy-start | bytes 98308
  7.2 5.9 %copy-start.11 = (f32[2048]{0:T(1024)S(1)}, f32[2048]{0:T(1024)}, u32[]{:S(2)}) copy-start(f32[2048]{0:T(1024)} %param.19) | copy-start | bytes 24580
  7.2 34.4 %all-gather.2.cloned.1.call-start = ((), (), s32[]{:S(2)}) async-start(), calls=%async_computation.1 | async-start | bytes 12681216 | tf_op jit(solution)/shard_map/all_gather | solution.py:183
  7.2 5.9 %copy-start.4 = (bf16[512,2,2048]{2,1,0:T(2,128)(2,1)S(1)}, bf16[512,2,2048]{2,1,0:T(2,128)(2,1)}, u32[]{:S(2)}) copy-start(bf16[512,2,2048]{2,1,0:T(2,128)(2,1)} %param.12) | copy-start | bytes 12582916
  41.6 12.8 %copy-start.14 = (bf16[2064,2048]{1,0:T(8,128)(2,1)S(1)}, bf16[2064,2048]{1,0:T(8,128)(2,1)}, u32[]{:S(2)}) copy-start(bf16[2064,2048]{1,0:T(8,128)(2,1)} %all-gather.2.cloned.1.call-done) | copy-start | bytes 25362436
  54.4 6.9 %copy-start.2 = (bf16[2064,1024]{1,0:T(8,128)(2,1)}, bf16[2064,1024]{1,0:T(8,128)(2,1)S(1)}, u32[]{:S(2)}) copy-start(bf16[2064,1024]{1,0:T(8,128)(2,1)S(1)} %convolution_convert_fusion.1) | copy-start | bytes 12681220
  54.5 8.8 %copy-start.15 = (bf16[2048,512]{1,0:T(8,128)(2,1)S(1)}, bf16[2048,512]{1,0:T(8,128)(2,1)}, u32[]{:S(2)}) copy-start(bf16[2048,512]{1,0:T(8,128)(2,1)} %param.15) | copy-start | bytes 6291460
  87.7 25.2 %collective-permute-start = (bf16[4,128,256]{2,1,0:T(8,128)(2,1)S(1)}, bf16[4,128,256]{2,1,0:T(8,128)(2,1)S(1)}, u32[]{:S(2)}, u32[]{:S(2)}) collective-permute-start(bf16[4,128,256]{2,1,0:T(8,128)(2,1)S(1)} %get-tuple-element.12), channel_id=1, source_target_pairs={{0,2},{2,4},{4,6},{1,3},{3,5},{5,7},{8,10},{10,12},{12,14},{9,11},... | collective-permute-start | bytes 786440 | tf_op jit(solution)/shard_map/ppermute | solution.py:152
  91.3 21.5 %collective-permute-start.3 = (bf16[4,128,256]{2,1,0:T(8,128)(2,1)S(1)}, bf16[4,128,256]{2,1,0:T(8,128)(2,1)S(1)}, u32[]{:S(2)}, u32[]{:S(2)}) collective-permute-start(bf16[4,128,256]{2,1,0:T(8,128)(2,1)S(1)} %get-tuple-element.13), channel_id=1, source_target_pairs={{0,2},{2,4},{4,6},{1,3},{3,5},{5,7},{8,10},{10,12},{12,14},{9,11},... | collective-permute-start | bytes 786440 | tf_op jit(solution)/shard_map/ppermute | solution.py:152
  95.1 8.1 %copy-start.16 = (bf16[2048,512]{1,0:T(8,128)(2,1)S(1)}, bf16[2048,512]{1,0:T(8,128)(2,1)}, u32[]{:S(2)}) copy-start(bf16[2048,512]{1,0:T(8,128)(2,1)} %param.14) | copy-start | bytes 6291460
  103.2 9.7 %copy-start.5 = (f32[2,4,128,256]{3,2,1,0:T(8,128)S(1)}, f32[2,4,128,256]{3,2,1,0:T(8,128)}, u32[]{:S(2)}) copy-start(f32[2,4,128,256]{3,2,1,0:T(8,128)} %get-tuple-element.7) | copy-start | bytes 3145732
  113.1 11.9 %collective-permute-start.1 = (bf16[4,128,256]{2,1,0:T(8,128)(2,1)S(1)}, bf16[4,128,256]{2,1,0:T(8,128)(2,1)S(1)}, u32[]{:S(2)}, u32[]{:S(2)}) collective-permute-start(bf16[4,128,256]{2,1,0:T(8,128)(2,1)S(1)} %get-tuple-element.10), channel_id=1, source_target_pairs={{0,2},{2,4},{4,6},{1,3},{3,5},{5,7},{8,10},{10,12},{12,14},{9,11},... | collective-permute-start | bytes 786440 | tf_op jit(solution)/shard_map/ppermute | solution.py:152
  116.5 11.0 %collective-permute-start.4 = (bf16[4,128,256]{2,1,0:T(8,128)(2,1)S(1)}, bf16[4,128,256]{2,1,0:T(8,128)(2,1)S(1)}, u32[]{:S(2)}, u32[]{:S(2)}) collective-permute-start(bf16[4,128,256]{2,1,0:T(8,128)(2,1)S(1)} %get-tuple-element.11), channel_id=1, source_target_pairs={{0,2},{2,4},{4,6},{1,3},{3,5},{5,7},{8,10},{10,12},{12,14},{9,11},... | collective-permute-start | bytes 786440 | tf_op jit(solution)/shard_map/ppermute | solution.py:152
  128.5 11.4 %collective-permute-start.2 = (bf16[4,128,256]{2,1,0:T(8,128)(2,1)}, bf16[4,128,256]{2,1,0:T(8,128)(2,1)S(1)}, u32[]{:S(2)}, u32[]{:S(2)}) collective-permute-start(bf16[4,128,256]{2,1,0:T(8,128)(2,1)} %get-tuple-element.8), channel_id=1, source_target_pairs={{0,2},{2,4},{4,6},{1,3},{3,5},{5,7},{8,10},{10,12},{12,14},{9,11},... | collective-permute-start | bytes 786440 | tf_op jit(solution)/shard_map/ppermute | solution.py:152
  132.9 10.4 %collective-permute-start.5 = (bf16[4,128,256]{2,1,0:T(8,128)(2,1)S(1)}, bf16[4,128,256]{2,1,0:T(8,128)(2,1)}, u32[]{:S(2)}, u32[]{:S(2)}) collective-permute-start(bf16[4,128,256]{2,1,0:T(8,128)(2,1)S(1)} %get-tuple-element.9), channel_id=1, source_target_pairs={{0,2},{2,4},{4,6},{1,3},{3,5},{5,7},{8,10},{10,12},{12,14},{9,11},... | collective-permute-start | bytes 786440 | tf_op jit(solution)/shard_map/ppermute | solution.py:152
  145.7 73.4 %copy-start.7 = (bf16[2,4,128,256]{3,2,1,0:T(8,128)(2,1)}, bf16[2,4,128,256]{3,2,1,0:T(8,128)(2,1)S(1)}, u32[]{:S(2)}) copy-start(bf16[2,4,128,256]{3,2,1,0:T(8,128)(2,1)S(1)} %get-tuple-element.14) | copy-start | bytes 1572868
  145.7 22.3 %copy-start.10 = (f32[1024]{0:T(1024)S(1)}, f32[1024]{0:T(1024)}, u32[]{:S(2)}) copy-start(f32[1024]{0:T(1024)} %dynamic_slice.7) | copy-start | bytes 12292
  177.2 45.6 %slice-start = ((s8[8388608]{0:T(1024)(128)(4,1)}), s8[4194304]{0:T(1024)(128)(4,1)S(1)}, s32[]{:S(2)}) async-start(s8[8388608]{0:T(1024)(128)(4,1)} %bitcast.110), calls=%async_computation.2 | async-start | bytes 8388608
  217.4 5.4 %slice-start.1 = ((s8[8388608]{0:T(1024)(128)(4,1)}), s8[4194304]{0:T(1024)(128)(4,1)S(1)}, s32[]{:S(2)}) async-start(s8[8388608]{0:T(1024)(128)(4,1)} %bitcast.110), calls=%async_computation.3 | async-start | bytes 8388608
  219.9 19.7 %collective-permute-start.6 = (bf16[2,4,32,256]{3,2,1,0:T(8,128)(2,1)}, bf16[2,4,32,256]{3,2,1,0:T(8,128)(2,1)S(1)}, u32[]{:S(2)}, u32[]{:S(2)}) collective-permute-start(bf16[2,4,32,256]{3,2,1,0:T(8,128)(2,1)} %get-tuple-element.18), channel_id=1, source_target_pairs={{6,4},{7,5},{14,12},{15,13},{22,20},{23,21},{30,28},{31,29}} | collective-permute-start | bytes 393224 | tf_op jit(solution)/shard_map/ppermute | solution.py:249
  220.6 19.1 %collective-permute-start.7 = (bf16[2,4,32,256]{3,2,1,0:T(8,128)(2,1)}, bf16[2,4,32,256]{3,2,1,0:T(8,128)(2,1)S(1)}, u32[]{:S(2)}, u32[]{:S(2)}) collective-permute-start(bf16[2,4,32,256]{3,2,1,0:T(8,128)(2,1)} %get-tuple-element.17), channel_id=1, source_target_pairs={{6,2},{7,3},{14,10},{15,11},{22,18},{23,19},{30,26},{31,27}} | collective-permute-start | bytes 393224 | tf_op jit(solution)/shard_map/ppermute | solution.py:249
  221.2 18.4 %collective-permute-start.8 = (bf16[2,4,32,256]{3,2,1,0:T(8,128)(2,1)S(1)}, bf16[2,4,32,256]{3,2,1,0:T(8,128)(2,1)}, u32[]{:S(2)}, u32[]{:S(2)}) collective-permute-start(bf16[2,4,32,256]{3,2,1,0:T(8,128)(2,1)S(1)} %get-tuple-element.16), channel_id=1, source_target_pairs={{6,0},{7,1},{14,8},{15,9},{22,16},{23,17},{30,24},{31,25}} | collective-permute-start | bytes 393224 | tf_op jit(solution)/shard_map/ppermute | solution.py:249
  233.3 8.1 %copy-start.1 = (bf16[2048,512]{1,0:T(8,128)(2,1)S(1)}, bf16[2048,512]{1,0:T(8,128)(2,1)}, u32[]{:S(2)}) copy-start(bf16[2048,512]{1,0:T(8,128)(2,1)} %param.17) | copy-start | bytes 6291460
  (5 other events, 6.3 us)
Sparse Core Ops, SparseCore 0:
  18.2 23.3 all-gather.1
